TPU v7x, 256 devices: a whole 4x4x8 slice. The times are simulated.
256 devices in a mesh: ep: 64 (over z, y, core), tp: 4 (over x).
Axes of the slice: x: 4, y: 4, z: 8, core: 2. Of those that a mesh axis runs over, the one named last changes fastest.
Arguments:
- cell_query_rows: bfloat16 [16384, 2048], P('ep', 'tp'), may hold values from -6 to 6
- cell_key_rows: bfloat16 [16384, 2048], P('ep', 'tp'), may hold values from -6 to 6
- cell_value_rows: bfloat16 [16384, 2048], P('ep', 'tp'), may hold values from -6 to 6
- output_gate_logits: bfloat16 [16384, 2048], P('ep', 'tp'), may hold values from -8 to 8
- log_input_gate: float32 [8, 16384], P('tp', 'ep'), may hold values from -4 to 110
- forget_gate_logits: float32 [8, 16384], P('tp', 'ep'), may hold values from -1 to 25
- extra_log_forget: float32 [8, 16384], P('tp', 'ep'), may hold values from -0.7 to 0
- cell_output_scale: float32 [2048], P('tp'), may hold values from 0.1 to 1.9
- tokens_into_experts: bfloat16 [32768, 2048], P(('ep', 'tp')), may hold values from -6 to 6
- expert_norm_scale: float32 [2048], replicated, may hold values from 0.1 to 1.9
- token_expert_index: int32 [32768, 2], P(('ep', 'tp')), may hold values from 0 to 63, all different within a row; in each aligned block of 128 rows (0 to 127, 128 to 255, ...) at most 5 rows name the same one
- chosen_expert_weight: float32 [32768, 2], P(('ep', 'tp')), may hold values from 0.3 to 3
- expert_gate_weight: bfloat16 [64, 2048, 3584], P('ep', None, 'tp'), may hold values from -0.125 to 0.125
- expert_up_weight: bfloat16 [64, 2048, 3584], P('ep', None, 'tp'), may hold values from -0.125 to 0.125
- expert_down_weight: bfloat16 [64, 3584, 2048], P('ep', 'tp'), may hold values from -0.09375 to 0.09375
Outputs:
- gated_head_output: bfloat16 [16384, 2048], P('ep', 'tp')
- expert_output: bfloat16 [32768, 2048], P(('ep', 'tp'))
Inputs may be any that keep to these rules, and one draw needn't show every extreme that they name: `token_expert_index`: each row names 2 different experts. Among the rows of one device (aligned blocks of 128 rows) no expert is named by more than 5 rows, and in every draw some expert is named by exactly 5 rows of some device.
All inputs are finite; a program needn't handle non-finite values.
Results may differ from a plain program's by a relative error of at most 0.012.
Values may be sent and summed in bfloat16 or wider, within the bound.
No kernel may reach another device: no remote copies, remote signals or barrier semaphores. Data moves between devices by JAX's collectives and lax.ppermute only.
A program may use at most 128 MiB of HBM per device.

v0:
```python
import functools

import jax
import jax.numpy as jnp
from jax import lax
from jax.experimental import pallas as pl
from jax.experimental.pallas import tpu as pltpu
from jax.sharding import Mesh
from jax.sharding import PartitionSpec as P


HEAD_DIM = 256
TOPK = 2
EPSILON = 1e-06
FAR = 1e30
META = 16
LANES = 128
EXPERT_LIMIT = 30 << 20
PACKED = (256 + META, 256)
GROUPS = ((0, 3), (3, 5))
YC = ("z", "y", "c")
ALL = ("z", "y", "c", "x")
F32 = jnp.float32
BF16 = jnp.bfloat16


VMEM = pl.BlockSpec(memory_space=pltpu.VMEM)
SMEM = pl.BlockSpec(memory_space=pltpu.SMEM)


def call(body, out_shape, in_specs, scratch=(), flops=0, limit=16 << 20):
    many = isinstance(out_shape, (list, tuple))
    return pl.pallas_call(
        body,
        out_shape=out_shape,
        in_specs=in_specs,
        out_specs=[VMEM] * len(out_shape) if many else VMEM,
        scratch_shapes=list(scratch),
        cost_estimate=pl.CostEstimate(flops=flops, bytes_accessed=flops // 256, transcendentals=0),
        compiler_params=pltpu.CompilerParams(vmem_limit_bytes=limit),
    )


def shape(dims, dtype=BF16):
    return jax.ShapeDtypeStruct(dims, dtype)


def pack(ref, cell, norm, top, total):
    dim = cell.shape[0]
    dtype = ref.dtype
    ref[0:dim, :] = cell.astype(dtype)
    row = lax.broadcasted_iota(jnp.int32, (META, dim), 0)
    meta = jnp.zeros((META, dim), F32)
    for at, value in enumerate((norm, top, total)):
        value = jnp.broadcast_to(value, (1, dim))
        for term in range(3):
            part = value.astype(BF16).astype(F32)
            value = value - part
            meta = jnp.where(row == 3 * at + term, part, meta)
    ref[dim : dim + META, :] = meta.astype(dtype)


def unpack(ref):
    dim = ref.shape[1]
    meta = ref[dim : dim + META, :].astype(F32)
    values = [meta[3 * k : 3 * k + 1] + meta[3 * k + 1 : 3 * k + 2] + meta[3 * k + 2 : 3 * k + 3] for k in range(3)]
    return values


def matrix(ref):
    return ref[0 : ref.shape[1], :].astype(F32)


def flag(condition):
    return jnp.where(condition, 1.0, 0.0).astype(F32)


def joined(entries, start=None):
    levels = []
    for j, (at, included, _, top, _) in enumerate(entries):
        level = top
        for i, (other_at, other_included, _, _, total) in enumerate(entries):
            if i != j:
                level = level + total * (other_included * flag(other_at > at))
        levels.append(level * included + (included - 1.0) * FAR)
    total_all = sum(entry[4] * entry[1] for entry in entries)
    highest = functools.reduce(jnp.maximum, levels)
    if start is not None:
        highest = jnp.maximum(highest, total_all + start)
    weights = [jnp.exp(level - highest) * entry[1] for level, entry in zip(levels, entries)]
    norm = sum(weight * entry[2] for weight, entry in zip(weights, entries))
    return weights, norm, highest, total_all


def gate_terms(forget_ref, extra_ref, gate_ref, head):
    dim = forget_ref.shape[1]
    logits = forget_ref[pl.ds(head, 1), :]
    log_forget = (
        jnp.minimum(logits, 0.0) - jnp.log1p(jnp.exp(-jnp.abs(logits))) + extra_ref[pl.ds(head, 1), :]
    )
    gate_row = gate_ref[pl.ds(head, 1), :]
    row = lax.broadcasted_iota(jnp.int32, (dim, dim), 0)
    col = lax.broadcasted_iota(jnp.int32, (dim, dim), 1)
    spread = jnp.broadcast_to(log_forget, (dim, dim))
    forget_col = jnp.sum(jnp.where(row == col, spread, 0.0), axis=1, keepdims=True)
    cum_col = jnp.sum(jnp.where(col <= row, spread, 0.0), axis=1, keepdims=True)
    cum_row = jnp.sum(jnp.where(row <= col, forget_col, 0.0), axis=0, keepdims=True)
    gate_col = jnp.sum(jnp.where(row == col, jnp.broadcast_to(gate_row, (dim, dim)), 0.0), axis=1, keepdims=True)
    return cum_col, cum_row, gate_col, gate_row, row, col


def totals_body(where_ref, key_ref, value_ref, gate_ref, forget_ref, extra_ref, own_ref, other_ref):
    core = where_ref[2]
    n_pos = key_ref.shape[0]
    for head, ref in ((core, own_ref), (1 - core, other_ref)):
        cum_col, _, gate_col, _, _, _ = gate_terms(forget_ref, extra_ref, gate_ref, head)
        total = cum_col[n_pos - 1 : n_pos, :]
        growth = total - cum_col + gate_col
        top = jnp.max(growth, axis=0, keepdims=True)
        shares = jnp.exp(growth - top)
        lanes = pl.ds(pl.multiple_of(head * HEAD_DIM, HEAD_DIM), HEAD_DIM)
        keys = key_ref[:, lanes]
        weighted = value_ref[:, lanes].astype(F32) * (shares * HEAD_DIM**-0.5)
        high = weighted.astype(BF16)
        low = (weighted - high.astype(F32)).astype(BF16)
        turned = (((0,), (0,)), ((), ()))
        cell = lax.dot_general(keys, high, turned, preferred_element_type=F32)
        cell = cell + lax.dot_general(keys, low, turned, preferred_element_type=F32)
        norm = jnp.sum(keys.astype(F32) * (shares * HEAD_DIM**-0.5), axis=0, keepdims=True)
        pack(ref, cell, norm, top, total)


def chip_body(where_ref, own_ref, other_ref, sent_ref, kept_ref):
    core = where_ref[2]
    entries = [(core, 1.0, *unpack(own_ref)), (1 - core, 1.0, *unpack(other_ref))]
    weights, norm, top, total = joined(entries)
    cell = weights[0] * matrix(own_ref) + weights[1] * matrix(other_ref)
    for ref in (sent_ref, kept_ref):
        pack(ref, cell, norm, top, total)


def earlier_states(upper, got_ref, before_refs):
    listed = [(0, flag(upper == 1), *unpack(got_ref))]
    return listed + [(1, 1.0, *unpack(ref)) for ref in before_refs]


def double_body(axis, bit, where_ref, got_ref, whole_ref, *refs):
    before_refs, (sent_ref, kept_ref, before_out) = refs[:-3], refs[-3:]
    upper = (where_ref[axis] >> bit) & 1
    entries = [(upper, 1.0, *unpack(whole_ref)), (1 - upper, 1.0, *unpack(got_ref))]
    weights, norm, top, total = joined(entries)
    cell = weights[0] * matrix(whole_ref) + weights[1] * matrix(got_ref)
    for ref in (sent_ref, kept_ref):
        pack(ref, cell, norm, top, total)
    weights, norm, top, total = joined(earlier_states(upper, got_ref, before_refs))
    cell = sum(weight * matrix(ref) for weight, ref in zip(weights, (got_ref, *before_refs)))
    pack(before_out, cell, norm, top, total)


def prefix_body(axis, bit, where_ref, got_ref, before_ref, own_ref, other_ref, mine_ref, partner_ref):
    upper, core = (where_ref[axis] >> bit) & 1, where_ref[2]
    own, other, second = unpack(own_ref), unpack(other_ref), core.astype(F32)
    first = [a * (1.0 - second) + b * second for a, b in zip(own, other)]
    first_cell = matrix(own_ref) * (1.0 - second) + matrix(other_ref) * second
    for target, ref in ((core, mine_ref), (1 - core, partner_ref)):
        listed = earlier_states(upper, got_ref, (before_ref,)) + [(2, target.astype(F32), *first)]
        weights, norm, top, total = joined(listed, start=0.0)
        cell = weights[0] * matrix(got_ref) + weights[1] * matrix(before_ref) + weights[2] * first_cell
        pack(ref, cell, norm, top, total)


def outputs_body(
    where_ref,
    query_ref,
    key_ref,
    value_ref,
    open_ref,
    gate_ref,
    forget_ref,
    extra_ref,
    scale_ref,
    own_ref,
    other_ref,
    out_ref,
):
    core = where_ref[2]
    for head, state_ref in ((core, own_ref), (1 - core, other_ref)):
        cum_col, cum_row, _, gate_row, row, col = gate_terms(forget_ref, extra_ref, gate_ref, head)
        norm, top_in, _ = unpack(state_ref)
        dim = state_ref.shape[1]
        lanes = pl.ds(pl.multiple_of(head * HEAD_DIM, HEAD_DIM), HEAD_DIM)
        queries, keys, values = query_ref[:, lanes], key_ref[:, lanes], value_ref[:, lanes]
        inter_log = cum_col + top_in[:, 0:1]
        spread = jnp.where(col <= row, cum_col - cum_row + gate_row, -jnp.inf)
        row_top = jnp.maximum(inter_log, jnp.max(spread, axis=1, keepdims=True))
        inter = jnp.exp(inter_log - row_top)
        scores = lax.dot_general(queries, keys, (((1,), (1,)), ((), ())), preferred_element_type=F32)
        scores = scores * HEAD_DIM**-0.5 * jnp.exp(spread - row_top)
        numerator = jnp.dot(scores.astype(BF16), values, preferred_element_type=F32)
        numerator = numerator + inter * jnp.dot(queries, state_ref[0:dim, :], preferred_element_type=F32)
        met = jnp.sum(queries.astype(F32) * norm, axis=1, keepdims=True)
        denominator = jnp.sum(scores, axis=1, keepdims=True) + inter * met
        cell_out = numerator / jnp.maximum(jnp.abs(denominator), 1.0)
        opened = jax.nn.sigmoid(open_ref[:, lanes].astype(F32))
        out_ref[:, lanes] = (cell_out * scale_ref[:, lanes] * opened).astype(BF16)


def moved(x, axis, shift):
    size = lax.axis_size(axis)
    return lax.ppermute(x, axis, [(k, (k + shift) % size) for k in range(size)])


def flipped(x, axis, bit):
    return lax.ppermute(x, axis, [(k, k ^ (1 << bit)) for k in range(lax.axis_size(axis))])


def places(ids_ref, experts):
    n_tok = ids_ref.shape[0]
    ids = ids_ref[...]
    lane = lax.broadcasted_iota(jnp.int32, (n_tok, experts), 1)
    named = [ids[:, k : k + 1] == lane for k in range(TOPK)]
    both = sum(jnp.where(hit, 1.0, 0.0) for hit in named)
    row = lax.broadcasted_iota(jnp.int32, (n_tok, n_tok), 0)
    col = lax.broadcasted_iota(jnp.int32, (n_tok, n_tok), 1)
    earlier = jnp.where(col < row, 1.0, 0.0).astype(BF16)
    ranks = jnp.dot(earlier, both.astype(BF16), preferred_element_type=F32)
    return [
        (ids[:, k : k + 1], jnp.sum(jnp.where(named[k], ranks, 0.0), axis=1, keepdims=True).astype(jnp.int32))
        for k in range(TOPK)
    ]


def chosen(place, experts, low, high):
    index, rank = place
    per = high - low
    column = jnp.where((rank >= low) & (rank < high), index * per + rank - low, -1)
    lane = lax.broadcasted_iota(jnp.int32, (index.shape[0], experts * per), 1)
    return jnp.where(column == lane, 1.0, 0.0)


def dispatch_body(experts, groups, token_ref, scale_ref, ids_ref, *out_refs):
    tokens = token_ref[...].astype(F32)
    mean = jnp.mean(tokens * tokens, axis=-1, keepdims=True)
    normed = (tokens * lax.rsqrt(mean + EPSILON) * scale_ref[...]).astype(BF16)
    found = places(ids_ref, experts)
    for (low, high), out_ref in zip(groups, out_refs):
        taken = sum(chosen(place, experts, low, high) for place in found).astype(BF16)
        out_ref[...] = lax.dot_general(
            taken, normed, (((0,), (0,)), ((), ())), preferred_element_type=F32
        ).astype(BF16)


def gather_body(experts, low, high, ids_ref, weight_ref, result_ref, *refs):
    out_ref = refs[-1]
    found = places(ids_ref, experts)
    result = result_ref[...]
    total = refs[0][...] if len(refs) > 1 else None
    for k, place in enumerate(found):
        taken = chosen(place, experts, low, high).astype(BF16)
        part = weight_ref[:, k : k + 1] * jnp.dot(taken, result, preferred_element_type=F32)
        total = part if total is None else total + part
    out_ref[...] = total.astype(out_ref.dtype)


def expert_body(own, left, right, far, gate, up, down, *refs):
    outs, (rows, hidden, pairs, held, arrived) = refs[:4], refs[4:]
    count = own.shape[0]
    tiles = gate.shape[1] // LANES

    def halves(j):
        return [
            pltpu.make_async_copy(
                ref.at[:, pl.ds(pl.multiple_of(j * LANES, LANES), LANES)],
                pairs.at[:, pl.ds(pl.multiple_of((2 * j + k) * LANES, LANES), LANES)],
                arrived.at[2 * j + k],
            )
            for k, ref in enumerate((gate, up))
        ]

    last = pltpu.make_async_copy(down, held, arrived.at[2 * tiles])
    for j in range(tiles):
        for copy in halves(j):
            copy.start()
    last.start()
    for k, ref in enumerate((own, left, right, far)):
        rows[k * count : (k + 1) * count] = ref[...]

    def into(j, carry):
        for copy in halves(j):
            copy.wait()
        both = pairs[:, pl.ds(pl.multiple_of(2 * j * LANES, 2 * LANES), 2 * LANES)]
        both = jnp.dot(rows[...], both, preferred_element_type=F32)
        gate_out, up_out = both[:, :LANES], both[:, LANES:]
        columns = pl.ds(pl.multiple_of(j * LANES, LANES), LANES)
        hidden[:, columns] = (gate_out * jax.nn.sigmoid(gate_out) * up_out).astype(BF16)
        return carry

    lax.fori_loop(0, tiles, into, 0)
    last.wait()

    def out_of(j, carry):
        columns = pl.ds(pl.multiple_of(2 * j * LANES, 2 * LANES), 2 * LANES)
        result = jnp.dot(hidden[...], held[:, columns], preferred_element_type=F32).astype(BF16)
        for k, out in enumerate(outs):
            out[:, columns] = result[k * count : (k + 1) * count]
        return carry

    lax.fori_loop(0, down.shape[1] // (2 * LANES), out_of, 0)


def all_rows(block, way):
    from_left = moved(block, "x", 1)
    from_right = moved(block, "x", -1)
    far = moved(from_left if way > 0 else from_right, "x", way)
    return block, from_left, from_right, far


def expert_parts(rows, weights):
    count, wide = rows[0].shape
    part = weights[0].shape[1]
    return call(
        expert_body,
        [shape((count, wide))] * 4,
        [VMEM] * 4 + [pl.BlockSpec(memory_space=pltpu.HBM)] * 3,
        scratch=[
            pltpu.VMEM((4 * count, wide), BF16),
            pltpu.VMEM((4 * count, part), BF16),
            pltpu.VMEM((wide, 2 * part), BF16),
            pltpu.VMEM((part, wide), BF16),
            pltpu.SemaphoreType.DMA((2 * part // LANES + 1,)),
        ],
        flops=4 * count * 2 * wide * 3 * weights[0].shape[1],
        limit=EXPERT_LIMIT,
    )(*rows, *weights)


def added(*terms):
    return functools.reduce(jnp.add, [term.astype(F32) for term in terms]).astype(BF16)


def summed(parts, way):
    own, left, right, away = parts
    relay = moved(away, "x", way)
    low = moved(added(right, relay) if way > 0 else right, "x", 1)
    high = moved(left if way > 0 else added(left, relay), "x", -1)
    return added(own, low, high)


def exchanged(rows, devices):
    wide = rows.shape[1]
    flat = rows.reshape(devices, -1, 128)
    flat = lax.all_to_all(flat, YC, 0, 0, tiled=True)
    return flat.reshape(-1, wide)


def step(
    cell_query_rows,
    cell_key_rows,
    cell_value_rows,
    output_gate_logits,
    log_input_gate,
    forget_gate_logits,
    extra_log_forget,
    cell_output_scale,
    tokens_into_experts,
    expert_norm_scale,
    token_expert_index,
    chosen_expert_weight,
    expert_gate_weight,
    expert_up_weight,
    expert_down_weight,
):
    where = jnp.stack([lax.axis_index(name) for name in ALL]).astype(jnp.int32)
    gates = (log_input_gate, forget_gate_logits, extra_log_forget)
    experts = lax.axis_size(YC)
    n_tok, wide = tokens_into_experts.shape
    weights = (expert_gate_weight[0], expert_up_weight[0], expert_down_weight[0])
    blocks = call(
        functools.partial(dispatch_body, experts, GROUPS),
        [shape((experts * (high - low), wide)) for low, high in GROUPS],
        [VMEM] * 3,
        flops=1 << 28,
    )(tokens_into_experts, expert_norm_scale.reshape(1, -1), token_expert_index)

    def gathered(at, result, *total):
        low, high = GROUPS[at]
        last = at == len(GROUPS) - 1
        return call(
            functools.partial(gather_body, experts, low, high),
            shape((n_tok, wide), BF16 if last else F32),
            [VMEM] * (3 + len(total)),
            flops=1 << 28,
        )(token_expert_index, chosen_expert_weight, result, *total)

    packed, packed_wide = shape(PACKED), shape(PACKED, F32)
    first = exchanged(blocks[0], experts)
    own, other = call(totals_body, [packed] * 2, [SMEM] + [VMEM] * 5, flops=1 << 27)(
        where, cell_key_rows, cell_value_rows, *gates
    )
    other = flipped(other, "c", 0)
    sent, whole = call(chip_body, [packed, packed_wide], [SMEM] + [VMEM] * 2, flops=1 << 25)(where, own, other)
    before = ()
    bits = [(axis, bit) for axis in "yz" for bit in range(lax.axis_size(axis).bit_length() - 1)]
    for axis, bit in bits[:-1]:
        got = flipped(sent, axis, bit)
        sent, whole, *before = call(
            functools.partial(double_body, ALL.index(axis), bit),
            [packed, packed_wide, packed_wide],
            [SMEM] + [VMEM] * (2 + len(before)),
            flops=1 << 25,
        )(where, got, whole, *before)
    axis, bit = bits[-1]
    got = flipped(sent, axis, bit)
    mine, partner = call(
        functools.partial(prefix_body, ALL.index(axis), bit), [packed] * 2, [SMEM] + [VMEM] * 4, flops=1 << 26
    )(where, got, *before, own, other)
    arrived = flipped(partner, "c", 0)
    mixed = call(outputs_body, shape(cell_query_rows.shape), [SMEM] + [VMEM] * 10, flops=1 << 28)(
        where,
        cell_query_rows,
        cell_key_rows,
        cell_value_rows,
        output_gate_logits,
        *gates,
        cell_output_scale.reshape(1, -1),
        mine,
        arrived,
    )
    second = exchanged(blocks[1], experts)
    weights = [pltpu.with_memory_space_constraint(x, pltpu.HBM) for x in weights]
    sums = []
    for block, way in ((first, 1), (second, -1)):
        parts = expert_parts(all_rows(block, way), weights)
        sums.append(summed(parts, way))
    first_back = exchanged(sums[0], experts)
    second_back = exchanged(sums[1], experts)
    expert_output = gathered(1, second_back, gathered(0, first_back))
    return (mixed, expert_output)


def solution(mesh):
    devices = mesh.devices
    finer = Mesh(devices.reshape(-1, 4, 2, mesh.shape["tp"]), ALL)
    placed = (
        P(YC, "x"),
        P(YC, "x"),
        P(YC, "x"),
        P(YC, "x"),
        P("x", YC),
        P("x", YC),
        P("x", YC),
        P("x"),
        P(ALL, None),
        P(),
        P(ALL, None),
        P(ALL, None),
        P(YC, None, "x"),
        P(YC, None, "x"),
        P(YC, "x", None),
    )
    return jax.shard_map(step, mesh=finer, in_specs=placed, out_specs=(P(YC, "x"), P(ALL, None)), check_vma=False)
```

profile of v0, /device:TPU:8, one launch (start us, length us, event | category | flops | bytes accessed | tf_op | source)
XLA Modules:
  0.0 244.1 jit_solution(14903988756621213840)
XLA Ops:
  5.2 12.1 %all-to-all-start = ((bf16[64,32,128]{2,1,0:T(8,128)(2,1)}), bf16[64,32,128]{2,1,0:T(8,128)(2,1)S(1)}, u32[]{:S(2)}, u32[]{:S(2)}) async-start(bf16[64,32,128]{2,1,0:T(8,128)(2,1)} %reshape.36), calls=%async_computation | async-start | bytes 1048576 | tf_op jit(solution)/shard_map/all_to_all | solution.py:352
  18.5 16.3 %all-to-all-done = bf16[64,32,128]{2,1,0:T(8,128)(2,1)S(1)} async-done(((bf16[64,32,128]{2,1,0:T(8,128)(2,1)}), bf16[64,32,128]{2,1,0:T(8,128)(2,1)S(1)}, u32[]{:S(2)}, u32[]{:S(2)}) %all-to-all-start) | async-done | bytes 524320 | tf_op jit(solution)/shard_map/all_to_all | solution.py:352
  34.8 5.8 %all-to-all-start.2 = ((bf16[64,48,128]{2,1,0:T(8,128)(2,1)}), bf16[64,48,128]{2,1,0:T(8,128)(2,1)S(1)}, u32[]{:S(2)}, u32[]{:S(2)}) async-start(bf16[64,48,128]{2,1,0:T(8,128)(2,1)} %reshape.40), calls=%async_computation.2 | async-start | bytes 1572864 | tf_op jit(solution)/shard_map/all_to_all | solution.py:352
  40.9 2.8 %collective-permute-start.8 = (bf16[128,2048]{1,0:T(8,128)(2,1)S(1)}, bf16[128,2048]{1,0:T(8,128)(2,1)S(1)}, u32[]{:S(2)}, u32[]{:S(2)}) collective-permute-start(bf16[128,2048]{1,0:T(8,128)(2,1)S(1)} %reshape.37.own), channel_id=1, source_target_pairs={{0,3},{1,0},{2,1},{3,2},{4,7},{5,4},{6,5},{7,6},{8,11},{9,8},{10,9... | collective-permute-start | bytes 1572872 | tf_op jit(solution)/shard_map/ppermute | solution.py:210
  43.7 20.1 %all-to-all-done.2 = bf16[64,48,128]{2,1,0:T(8,128)(2,1)S(1)} async-done(((bf16[64,48,128]{2,1,0:T(8,128)(2,1)}), bf16[64,48,128]{2,1,0:T(8,128)(2,1)S(1)}, u32[]{:S(2)}, u32[]{:S(2)}) %all-to-all-start.2) | async-done | bytes 786464 | tf_op jit(solution)/shard_map/all_to_all | solution.py:352
  69.5 16.4 %collective-permute-done.13.left = bf16[192,2048]{1,0:T(8,128)(2,1)S(1)} collective-permute-done((bf16[192,2048]{1,0:T(8,128)(2,1)S(1)}, bf16[192,2048]{1,0:T(8,128)(2,1)S(1)}, u32[]{:S(2)}, u32[]{:S(2)}) %collective-permute-start.13) | collective-permute-done | bytes 786464 | tf_op jit(solution)/shard_map/ppermute | solution.py:210
  86.1 11.0 %collective-permute-done.7.left = bf16[128,2048]{1,0:T(8,128)(2,1)S(1)} collective-permute-done((bf16[128,2048]{1,0:T(8,128)(2,1)S(1)}, bf16[128,2048]{1,0:T(8,128)(2,1)S(1)}, u32[]{:S(2)}, u32[]{:S(2)}) %collective-permute-start.7) | collective-permute-done | bytes 524320 | tf_op jit(solution)/shard_map/ppermute | solution.py:210
  97.1 10.1 %shard_map.167 = (bf16[128,2048]{1,0:T(8,128)(2,1)S(1)}, bf16[128,2048]{1,0:T(8,128)(2,1)S(1)}, bf16[128,2048]{1,0:T(8,128)(2,1)S(1)}, bf16[128,2048]{1,0:T(8,128)(2,1)S(1)}) custom-call(bf16[128,2048]{1,0:T(8,128)(2,1)S(1)} %reshape.37.own, bf16[128,2048]{1,0:T(8,128)(2,1)S(1)} %collective-permute-done.7.left, ...), custom_call_target="tpu_custom_call" | custom-call | flops 5637144576 | bytes 22020096 | tf_op jit(solution)/shard_map/pallas_call | solution.py:321
  108.8 3.6 %collective-permute-done.15.far = bf16[192,2048]{1,0:T(8,128)(2,1)S(1)} collective-permute-done((bf16[192,2048]{1,0:T(8,128)(2,1)S(1)}, bf16[192,2048]{1,0:T(8,128)(2,1)S(1)}, u32[]{:S(2)}, u32[]{:S(2)}) %collective-permute-start.15) | collective-permute-done | bytes 786464 | tf_op jit(solution)/shard_map/ppermute | solution.py:210
  112.4 13.0 %shard_map.168 = (bf16[192,2048]{1,0:T(8,128)(2,1)S(1)}, bf16[192,2048]{1,0:T(8,128)(2,1)S(1)}, bf16[192,2048]{1,0:T(8,128)(2,1)S(1)}, bf16[192,2048]{1,0:T(8,128)(2,1)S(1)}) custom-call(bf16[192,2048]{1,0:T(8,128)(2,1)S(1)} %reshape.41.own, bf16[192,2048]{1,0:T(8,128)(2,1)S(1)} %collective-permute-done.13.left, ...), custom_call_target="tpu_custom_call" | custom-call | flops 8455716864 | bytes 33030144 | tf_op jit(solution)/shard_map/pallas_call | solution.py:321
  131.1 16.1 %collective-permute-done.16 = bf16[192,2048]{1,0:T(8,128)(2,1)S(1)} collective-permute-done((bf16[192,2048]{1,0:T(8,128)(2,1)S(1)}, bf16[192,2048]{1,0:T(8,128)(2,1)S(1)}, u32[]{:S(2)}, u32[]{:S(2)}) %collective-permute-start.16) | collective-permute-done | bytes 786464 | tf_op jit(solution)/shard_map/ppermute | solution.py:210
  148.4 10.1 %collective-permute-done.10 = bf16[128,2048]{1,0:T(8,128)(2,1)S(1)} collective-permute-done((bf16[128,2048]{1,0:T(8,128)(2,1)S(1)}, bf16[128,2048]{1,0:T(8,128)(2,1)S(1)}, u32[]{:S(2)}, u32[]{:S(2)}) %collective-permute-start.10) | collective-permute-done | bytes 524320 | tf_op jit(solution)/shard_map/ppermute | solution.py:210
  159.8 6.0 %all-to-all-start.1 = ((bf16[64,32,128]{2,1,0:T(8,128)(2,1)}), bf16[64,32,128]{2,1,0:T(8,128)(2,1)S(1)}, u32[]{:S(2)}, u32[]{:S(2)}) async-start(bf16[64,32,128]{2,1,0:T(8,128)(2,1)} %reshape.38), calls=%async_computation.1 | async-start | bytes 1048576 | tf_op jit(solution)/shard_map/all_to_all | solution.py:352
  165.8 7.3 %collective-permute-done.17 = bf16[192,2048]{1,0:T(8,128)(2,1)} collective-permute-done((bf16[192,2048]{1,0:T(8,128)(2,1)}, bf16[192,2048]{1,0:T(8,128)(2,1)}, u32[]{:S(2)}, u32[]{:S(2)}) %collective-permute-start.17) | collective-permute-done | bytes 786464 | tf_op jit(solution)/shard_map/ppermute | solution.py:210
  176.2 7.1 %all-to-all-done.1 = bf16[64,32,128]{2,1,0:T(8,128)(2,1)S(1)} async-done(((bf16[64,32,128]{2,1,0:T(8,128)(2,1)}), bf16[64,32,128]{2,1,0:T(8,128)(2,1)S(1)}, u32[]{:S(2)}, u32[]{:S(2)}) %all-to-all-start.1) | async-done | bytes 524320 | tf_op jit(solution)/shard_map/all_to_all | solution.py:352
  183.3 5.8 %all-to-all-start.3 = ((bf16[64,48,128]{2,1,0:T(8,128)(2,1)}), bf16[64,48,128]{2,1,0:T(8,128)(2,1)S(1)}, u32[]{:S(2)}, u32[]{:S(2)}) async-start(bf16[64,48,128]{2,1,0:T(8,128)(2,1)} %reshape.42), calls=%async_computation.3 | async-start | bytes 1572864 | tf_op jit(solution)/shard_map/all_to_all | solution.py:352
  193.2 8.0 %collective-permute-done.1.got_ref = bf16[272,256]{1,0:T(8,128)(2,1)S(1)} collective-permute-done((bf16[272,256]{1,0:T(8,128)(2,1)S(1)}, bf16[272,256]{1,0:T(8,128)(2,1)S(1)}, u32[]{:S(2)}, u32[]{:S(2)}) %collective-permute-start.1) | collective-permute-done | bytes 139296 | tf_op jit(solution)/shard_map/ppermute | solution.py:214
  203.5 7.3 %collective-permute-done.2.got_ref = bf16[272,256]{1,0:T(8,128)(2,1)S(1)} collective-permute-done((bf16[272,256]{1,0:T(8,128)(2,1)S(1)}, bf16[272,256]{1,0:T(8,128)(2,1)S(1)}, u32[]{:S(2)}, u32[]{:S(2)}) %collective-permute-start.2) | collective-permute-done | bytes 139296 | tf_op jit(solution)/shard_map/ppermute | solution.py:214
  212.0 4.6 %collective-permute-done.3.got_ref = bf16[272,256]{1,0:T(8,128)(2,1)S(1)} collective-permute-done((bf16[272,256]{1,0:T(8,128)(2,1)S(1)}, bf16[272,256]{1,0:T(8,128)(2,1)S(1)}, u32[]{:S(2)}, u32[]{:S(2)}) %collective-permute-start.3) | collective-permute-done | bytes 139296 | tf_op jit(solution)/shard_map/ppermute | solution.py:214
  217.3 2.6 %collective-permute-start.4 = (bf16[272,256]{1,0:T(8,128)(2,1)S(1)}, bf16[272,256]{1,0:T(8,128)(2,1)S(1)}, u32[]{:S(2)}, u32[]{:S(2)}) collective-permute-start(bf16[272,256]{1,0:T(8,128)(2,1)S(1)} %get-tuple-element.39), channel_id=1, source_target_pairs={{0,64},{32,96},{64,0},{96,32},{128,192},{160,224},{192,128},{224,1... | collective-permute-start | bytes 417800 | tf_op jit(solution)/shard_map/ppermute | solution.py:214
  219.9 5.5 %collective-permute-done.4.got_ref = bf16[272,256]{1,0:T(8,128)(2,1)S(1)} collective-permute-done((bf16[272,256]{1,0:T(8,128)(2,1)S(1)}, bf16[272,256]{1,0:T(8,128)(2,1)S(1)}, u32[]{:S(2)}, u32[]{:S(2)}) %collective-permute-start.4) | collective-permute-done | bytes 139296 | tf_op jit(solution)/shard_map/ppermute | solution.py:214
  226.7 3.9 %collective-permute-start.5 = (bf16[272,256]{1,0:T(8,128)(2,1)S(1)}, bf16[272,256]{1,0:T(8,128)(2,1)S(1)}, u32[]{:S(2)}, u32[]{:S(2)}) collective-permute-start(bf16[272,256]{1,0:T(8,128)(2,1)S(1)} %get-tuple-element.42), channel_id=1, source_target_pairs={{0,128},{32,160},{64,192},{96,224},{128,0},{160,32},{192,64},{224,... | collective-permute-start | bytes 417800 | tf_op jit(solution)/shard_map/ppermute | solution.py:214
  230.6 5.9 %collective-permute-done.5.got_ref = bf16[272,256]{1,0:T(8,128)(2,1)S(1)} collective-permute-done((bf16[272,256]{1,0:T(8,128)(2,1)S(1)}, bf16[272,256]{1,0:T(8,128)(2,1)S(1)}, u32[]{:S(2)}, u32[]{:S(2)}) %collective-permute-start.5) | collective-permute-done | bytes 139296 | tf_op jit(solution)/shard_map/ppermute | solution.py:214
  238.9 2.2 shard_map.165
  (72 shorter events, 39.7 us)
Async XLA Ops:
  5.2 29.6 %all-to-all-start = ((bf16[64,32,128]{2,1,0:T(8,128)(2,1)}), bf16[64,32,128]{2,1,0:T(8,128)(2,1)S(1)}, u32[]{:S(2)}, u32[]{:S(2)}) async-start(bf16[64,32,128]{2,1,0:T(8,128)(2,1)} %reshape.36), calls=%async_computation | async-start | bytes 1048576 | tf_op jit(solution)/shard_map/all_to_all | solution.py:352
  34.8 29.0 %all-to-all-start.2 = ((bf16[64,48,128]{2,1,0:T(8,128)(2,1)}), bf16[64,48,128]{2,1,0:T(8,128)(2,1)S(1)}, u32[]{:S(2)}, u32[]{:S(2)}) async-start(bf16[64,48,128]{2,1,0:T(8,128)(2,1)} %reshape.40), calls=%async_computation.2 | async-start | bytes 1572864 | tf_op jit(solution)/shard_map/all_to_all | solution.py:352
  40.9 26.3 %collective-permute-start.8 = (bf16[128,2048]{1,0:T(8,128)(2,1)S(1)}, bf16[128,2048]{1,0:T(8,128)(2,1)S(1)}, u32[]{:S(2)}, u32[]{:S(2)}) collective-permute-start(bf16[128,2048]{1,0:T(8,128)(2,1)S(1)} %reshape.37.own), channel_id=1, source_target_pairs={{0,3},{1,0},{2,1},{3,2},{4,7},{5,4},{6,5},{7,6},{8,11},{9,8},{10,9... | collective-permute-start | bytes 1572872 | tf_op jit(solution)/shard_map/ppermute | solution.py:210
  64.1 21.7 %collective-permute-start.13 = (bf16[192,2048]{1,0:T(8,128)(2,1)S(1)}, bf16[192,2048]{1,0:T(8,128)(2,1)S(1)}, u32[]{:S(2)}, u32[]{:S(2)}) collective-permute-start(bf16[192,2048]{1,0:T(8,128)(2,1)S(1)} %reshape.41.own), channel_id=1, source_target_pairs={{0,1},{1,2},{2,3},{3,0},{4,5},{5,6},{6,7},{7,4},{8,9},{9,10},{10,1... | collective-permute-start | bytes 2359304 | tf_op jit(solution)/shard_map/ppermute | solution.py:210
  65.7 31.4 %collective-permute-start.7 = (bf16[128,2048]{1,0:T(8,128)(2,1)S(1)}, bf16[128,2048]{1,0:T(8,128)(2,1)S(1)}, u32[]{:S(2)}, u32[]{:S(2)}) collective-permute-start(bf16[128,2048]{1,0:T(8,128)(2,1)S(1)} %reshape.37.own), channel_id=1, source_target_pairs={{0,1},{1,2},{2,3},{3,0},{4,5},{5,6},{6,7},{7,4},{8,9},{9,10},{10,1... | collective-permute-start | bytes 1572872 | tf_op jit(solution)/shard_map/ppermute | solution.py:210
  67.2 29.9 %collective-permute-start.9 = (bf16[128,2048]{1,0:T(8,128)(2,1)S(1)}, bf16[128,2048]{1,0:T(8,128)(2,1)S(1)}, u32[]{:S(2)}, u32[]{:S(2)}) collective-permute-start(bf16[128,2048]{1,0:T(8,128)(2,1)S(1)} %collective-permute-done.8.right), channel_id=1, source_target_pairs={{0,3},{1,0},{2,1},{3,2},{4,7},{5,4},{6,5},{7,6},{8,11},{9,8},{10,9... | collective-permute-start | bytes 1572872 | tf_op jit(solution)/shard_map/ppermute | solution.py:210
  69.0 39.9 %collective-permute-start.14 = (bf16[192,2048]{1,0:T(8,128)(2,1)S(1)}, bf16[192,2048]{1,0:T(8,128)(2,1)S(1)}, u32[]{:S(2)}, u32[]{:S(2)}) collective-permute-start(bf16[192,2048]{1,0:T(8,128)(2,1)S(1)} %reshape.41.own), channel_id=1, source_target_pairs={{0,3},{1,0},{2,1},{3,2},{4,7},{5,4},{6,5},{7,6},{8,11},{9,8},{10,9... | collective-permute-start | bytes 2359304 | tf_op jit(solution)/shard_map/ppermute | solution.py:210
  85.8 26.6 %collective-permute-start.15 = (bf16[192,2048]{1,0:T(8,128)(2,1)S(1)}, bf16[192,2048]{1,0:T(8,128)(2,1)S(1)}, u32[]{:S(2)}, u32[]{:S(2)}) collective-permute-start(bf16[192,2048]{1,0:T(8,128)(2,1)S(1)} %collective-permute-done.13.left), channel_id=1, source_target_pairs={{0,1},{1,2},{2,3},{3,0},{4,5},{5,6},{6,7},{7,4},{8,9},{9,10},{10,1... | collective-permute-start | bytes 2359304 | tf_op jit(solution)/shard_map/ppermute | solution.py:210
  107.2 20.2 %collective-permute-start.11 = (bf16[128,2048]{1,0:T(8,128)(2,1)S(1)}, bf16[128,2048]{1,0:T(8,128)(2,1)S(1)}, u32[]{:S(2)}, u32[]{:S(2)}) collective-permute-start(bf16[128,2048]{1,0:T(8,128)(2,1)S(1)} %get-tuple-element.50), channel_id=1, source_target_pairs={{0,3},{1,0},{2,1},{3,2},{4,7},{5,4},{6,5},{7,6},{8,11},{9,8},{10,9... | collective-permute-start | bytes 1572872 | tf_op jit(solution)/shard_map/ppermute | solution.py:210
  125.4 21.9 %collective-permute-start.16 = (bf16[192,2048]{1,0:T(8,128)(2,1)S(1)}, bf16[192,2048]{1,0:T(8,128)(2,1)S(1)}, u32[]{:S(2)}, u32[]{:S(2)}) collective-permute-start(bf16[192,2048]{1,0:T(8,128)(2,1)S(1)} %get-tuple-element.54), channel_id=1, source_target_pairs={{0,1},{1,2},{2,3},{3,0},{4,5},{5,6},{6,7},{7,4},{8,9},{9,10},{10,1... | collective-permute-start | bytes 2359304 | tf_op jit(solution)/shard_map/ppermute | solution.py:210
  125.9 32.6 %collective-permute-start.10 = (bf16[128,2048]{1,0:T(8,128)(2,1)S(1)}, bf16[128,2048]{1,0:T(8,128)(2,1)S(1)}, u32[]{:S(2)}, u32[]{:S(2)}) collective-permute-start(bf16[128,2048]{1,0:T(8,128)(2,1)S(1)} %get-tuple-element.48), channel_id=1, source_target_pairs={{0,1},{1,2},{2,3},{3,0},{4,5},{5,6},{6,7},{7,4},{8,9},{9,10},{10,1... | collective-permute-start | bytes 1572872 | tf_op jit(solution)/shard_map/ppermute | solution.py:210
  127.5 31.0 %collective-permute-start.12 = (bf16[128,2048]{1,0:T(8,128)(2,1)S(1)}, bf16[128,2048]{1,0:T(8,128)(2,1)S(1)}, u32[]{:S(2)}, u32[]{:S(2)}) collective-permute-start(bf16[128,2048]{1,0:T(8,128)(2,1)S(1)} %add_convert_fusion.3), channel_id=1, source_target_pairs={{0,3},{1,0},{2,1},{3,2},{4,7},{5,4},{6,5},{7,6},{8,11},{9,8},{10,9... | collective-permute-start | bytes 1572872 | tf_op jit(solution)/shard_map/ppermute | solution.py:210
  129.4 36.4 %collective-permute-start.18 = (bf16[192,2048]{1,0:T(8,128)(2,1)S(1)}, bf16[192,2048]{1,0:T(8,128)(2,1)}, u32[]{:S(2)}, u32[]{:S(2)}) collective-permute-start(bf16[192,2048]{1,0:T(8,128)(2,1)S(1)} %get-tuple-element.55), channel_id=1, source_target_pairs={{0,3},{1,0},{2,1},{3,2},{4,7},{5,4},{6,5},{7,6},{8,11},{9,8},{10,9... | collective-permute-start | bytes 2359304 | tf_op jit(solution)/shard_map/ppermute | solution.py:210
  148.4 24.6 %collective-permute-start.17 = (bf16[192,2048]{1,0:T(8,128)(2,1)}, bf16[192,2048]{1,0:T(8,128)(2,1)}, u32[]{:S(2)}, u32[]{:S(2)}) collective-permute-start(bf16[192,2048]{1,0:T(8,128)(2,1)} %add_convert_fusion.1), channel_id=1, source_target_pairs={{0,1},{1,2},{2,3},{3,0},{4,5},{5,6},{6,7},{7,4},{8,9},{9,10},{10,1... | collective-permute-start | bytes 2359304 | tf_op jit(solution)/shard_map/ppermute | solution.py:210
  159.8 23.5 %all-to-all-start.1 = ((bf16[64,32,128]{2,1,0:T(8,128)(2,1)}), bf16[64,32,128]{2,1,0:T(8,128)(2,1)S(1)}, u32[]{:S(2)}, u32[]{:S(2)}) async-start(bf16[64,32,128]{2,1,0:T(8,128)(2,1)} %reshape.38), calls=%async_computation.1 | async-start | bytes 1048576 | tf_op jit(solution)/shard_map/all_to_all | solution.py:352
  183.3 58.0 %all-to-all-start.3 = ((bf16[64,48,128]{2,1,0:T(8,128)(2,1)}), bf16[64,48,128]{2,1,0:T(8,128)(2,1)S(1)}, u32[]{:S(2)}, u32[]{:S(2)}) async-start(bf16[64,48,128]{2,1,0:T(8,128)(2,1)} %reshape.42), calls=%async_computation.3 | async-start | bytes 1572864 | tf_op jit(solution)/shard_map/all_to_all | solution.py:352
  190.5 1.4 collective-permute-start
  192.6 8.6 %collective-permute-start.1 = (bf16[272,256]{1,0:T(8,128)(2,1)S(1)}, bf16[272,256]{1,0:T(8,128)(2,1)S(1)}, u32[]{:S(2)}, u32[]{:S(2)}) collective-permute-start(bf16[272,256]{1,0:T(8,128)(2,1)S(1)} %get-tuple-element.31), channel_id=1, source_target_pairs={{0,8},{8,0},{16,24},{24,16},{1,9},{9,1},{17,25},{25,17},{2,10},{10... | collective-permute-start | bytes 417800 | tf_op jit(solution)/shard_map/ppermute | solution.py:214
  201.2 37.8 %copy-start.7 = (f32[512]{0:T(512)S(1)}, f32[512]{0:T(512)}, u32[]{:S(2)}) copy-start(f32[512]{0:T(512)} %param.22) | copy-start | bytes 6148
  201.9 8.9 %collective-permute-start.2 = (bf16[272,256]{1,0:T(8,128)(2,1)S(1)}, bf16[272,256]{1,0:T(8,128)(2,1)S(1)}, u32[]{:S(2)}, u32[]{:S(2)}) collective-permute-start(bf16[272,256]{1,0:T(8,128)(2,1)S(1)} %get-tuple-element.33), channel_id=1, source_target_pairs={{0,16},{8,24},{16,0},{24,8},{1,17},{9,25},{17,1},{25,9},{2,18},{10... | collective-permute-start | bytes 417800 | tf_op jit(solution)/shard_map/ppermute | solution.py:214
  211.4 5.1 %collective-permute-start.3 = (bf16[272,256]{1,0:T(8,128)(2,1)S(1)}, bf16[272,256]{1,0:T(8,128)(2,1)S(1)}, u32[]{:S(2)}, u32[]{:S(2)}) collective-permute-start(bf16[272,256]{1,0:T(8,128)(2,1)S(1)} %get-tuple-element.36), channel_id=1, source_target_pairs={{0,32},{32,0},{64,96},{96,64},{128,160},{160,128},{192,224},{224,1... | collective-permute-start | bytes 417800 | tf_op jit(solution)/shard_map/ppermute | solution.py:214
  217.3 8.1 %collective-permute-start.4 = (bf16[272,256]{1,0:T(8,128)(2,1)S(1)}, bf16[272,256]{1,0:T(8,128)(2,1)S(1)}, u32[]{:S(2)}, u32[]{:S(2)}) collective-permute-start(bf16[272,256]{1,0:T(8,128)(2,1)S(1)} %get-tuple-element.39), channel_id=1, source_target_pairs={{0,64},{32,96},{64,0},{96,32},{128,192},{160,224},{192,128},{224,1... | collective-permute-start | bytes 417800 | tf_op jit(solution)/shard_map/ppermute | solution.py:214
  226.7 9.8 %collective-permute-start.5 = (bf16[272,256]{1,0:T(8,128)(2,1)S(1)}, bf16[272,256]{1,0:T(8,128)(2,1)S(1)}, u32[]{:S(2)}, u32[]{:S(2)}) collective-permute-start(bf16[272,256]{1,0:T(8,128)(2,1)S(1)} %get-tuple-element.42), channel_id=1, source_target_pairs={{0,128},{32,160},{64,192},{96,224},{128,0},{160,32},{192,64},{224,... | collective-permute-start | bytes 417800 | tf_op jit(solution)/shard_map/ppermute | solution.py:214
  237.3 1.7 collective-permute-start.6
  (10 other events, 185.6 us)
where the time goes:
time: 247 us; the launch traced here: 244 us
  waiting for transfers between devices  142 us (57%)
  starting transfers between devices  55.2 us (22%)
  Pallas kernels  34.6 us (14%)
  local copies, waits for them, and re-layouts  8.39 us (3%)
  other arithmetic  3.37 us (1%)
    ppermute x12, waiting for transfers between devices, moved(): return lax.ppermute(x, axis, [(k, (k + shift) % size) for k in range(size)])  64.4 us
    all_to_all x4, waiting for transfers between devices, exchanged(): flat = lax.all_to_all(flat, YC, 0, 0, tiled=True)  43.5 us
    ppermute x7, waiting for transfers between devices, flipped(): lax.ppermute(x, axis, [(k, k ^ 1 << bit) for k in range(lax.axis_size(axi...  33.7 us
    all_to_all x4, starting transfers between devices, exchanged(): flat = lax.all_to_all(flat, YC, 0, 0, tiled=True)  29.8 us
    pallas_call x2, Pallas kernels, expert_parts(): call(expert_body, [shape((count, wide))] * 4, [VMEM] * 4 + [pl.BlockSpec(...  23.1 us
    ppermute x12, starting transfers between devices, moved(): return lax.ppermute(x, axis, [(k, (k + shift) % size) for k in range(size)])  15.7 us
    ppermute x7, starting transfers between devices, flipped(): lax.ppermute(x, axis, [(k, k ^ 1 << bit) for k in range(lax.axis_size(axi...  9.76 us
  transfers between devices with their start and end apart: 23, of which 16 were waited for; matrix products, arithmetic and copies ran while one was open for 3% of the time, Pallas kernels for 13%

commit v1 on v0

--- a/solution.py
+++ b/solution.py
@@ -15,9 +15,11 @@
 FAR = 1e30
 META = 16
 LANES = 128
-EXPERT_LIMIT = 30 << 20
+EXPERT_LIMIT = 16 << 20
+JOIN_FLOPS = 1 << 33
 PACKED = (256 + META, 256)
-GROUPS = ((0, 3), (3, 5))
+GROUPS = ((0, 2), (2, 5))
+WAYS = (1, 0)
 YC = ("z", "y", "c")
 ALL = ("z", "y", "c", "x")
 F32 = jnp.float32
@@ -214,19 +216,27 @@
     return lax.ppermute(x, axis, [(k, k ^ (1 << bit)) for k in range(lax.axis_size(axis))])
 
 
+def upright(row_values):
+    count = row_values.shape[1]
+    row = lax.broadcasted_iota(jnp.int32, (count, count), 0)
+    col = lax.broadcasted_iota(jnp.int32, (count, count), 1)
+    spread = jnp.broadcast_to(row_values, (count, count))
+    return jnp.sum(jnp.where(row == col, spread, 0.0), axis=1, keepdims=True)
+
+
 def places(ids_ref, experts):
-    n_tok = ids_ref.shape[0]
-    ids = ids_ref[...]
+    n_tok = ids_ref.shape[1]
+    ids = [upright(ids_ref[k : k + 1, :].astype(F32)).astype(jnp.int32) for k in range(TOPK)]
     lane = lax.broadcasted_iota(jnp.int32, (n_tok, experts), 1)
-    named = [ids[:, k : k + 1] == lane for k in range(TOPK)]
+    named = [index == lane for index in ids]
     both = sum(jnp.where(hit, 1.0, 0.0) for hit in named)
     row = lax.broadcasted_iota(jnp.int32, (n_tok, n_tok), 0)
     col = lax.broadcasted_iota(jnp.int32, (n_tok, n_tok), 1)
     earlier = jnp.where(col < row, 1.0, 0.0).astype(BF16)
     ranks = jnp.dot(earlier, both.astype(BF16), preferred_element_type=F32)
     return [
-        (ids[:, k : k + 1], jnp.sum(jnp.where(named[k], ranks, 0.0), axis=1, keepdims=True).astype(jnp.int32))
-        for k in range(TOPK)
+        (index, jnp.sum(jnp.where(hit, ranks, 0.0), axis=1, keepdims=True).astype(jnp.int32))
+        for index, hit in zip(ids, named)
     ]
 
 
@@ -238,11 +248,20 @@
     return jnp.where(column == lane, 1.0, 0.0)
 
 
-def dispatch_body(experts, groups, token_ref, scale_ref, ids_ref, *out_refs):
-    tokens = token_ref[...].astype(F32)
+def dispatch_body(experts, groups, token_ref, scale_ref, ids_ref, *refs):
+    out_refs, (held, scale, arrived) = refs[: len(groups)], refs[len(groups) :]
+    copies = [
+        pltpu.make_async_copy(token_ref, held, arrived.at[0]),
+        pltpu.make_async_copy(scale_ref, scale, arrived.at[1]),
+    ]
+    for copy in copies:
+        copy.start()
+    found = places(ids_ref, experts)
+    for copy in copies:
+        copy.wait()
+    tokens = held[...].astype(F32)
     mean = jnp.mean(tokens * tokens, axis=-1, keepdims=True)
-    normed = (tokens * lax.rsqrt(mean + EPSILON) * scale_ref[...]).astype(BF16)
-    found = places(ids_ref, experts)
+    normed = (tokens * lax.rsqrt(mean + EPSILON) * scale[...]).astype(BF16)
     for (low, high), out_ref in zip(groups, out_refs):
         taken = sum(chosen(place, experts, low, high) for place in found).astype(BF16)
         out_ref[...] = lax.dot_general(
@@ -257,93 +276,91 @@
     total = refs[0][...] if len(refs) > 1 else None
     for k, place in enumerate(found):
         taken = chosen(place, experts, low, high).astype(BF16)
-        part = weight_ref[:, k : k + 1] * jnp.dot(taken, result, preferred_element_type=F32)
+        part = upright(weight_ref[k : k + 1, :]) * jnp.dot(taken, result, preferred_element_type=F32)
         total = part if total is None else total + part
     out_ref[...] = total.astype(out_ref.dtype)
 
 
-def expert_body(own, left, right, far, gate, up, down, *refs):
-    outs, (rows, hidden, pairs, held, arrived) = refs[:4], refs[4:]
-    count = own.shape[0]
-    tiles = gate.shape[1] // LANES
-
-    def halves(j):
-        return [
-            pltpu.make_async_copy(
-                ref.at[:, pl.ds(pl.multiple_of(j * LANES, LANES), LANES)],
-                pairs.at[:, pl.ds(pl.multiple_of((2 * j + k) * LANES, LANES), LANES)],
-                arrived.at[2 * j + k],
-            )
-            for k, ref in enumerate((gate, up))
-        ]
-
-    last = pltpu.make_async_copy(down, held, arrived.at[2 * tiles])
-    for j in range(tiles):
-        for copy in halves(j):
-            copy.start()
-    last.start()
-    for k, ref in enumerate((own, left, right, far)):
-        rows[k * count : (k + 1) * count] = ref[...]
+def expert_body(n_in, *refs):
+    ins, (gates, ups, downs), refs = refs[:n_in], refs[n_in : n_in + 3], refs[n_in + 3 :]
+    outs, (rows, hidden) = refs[:n_in], refs[n_in:]
+    at = 0
+    for ref in ins:
+        rows[at : at + ref.shape[0]] = ref[...]
+        at += ref.shape[0]
 
     def into(j, carry):
-        for copy in halves(j):
-            copy.wait()
-        both = pairs[:, pl.ds(pl.multiple_of(2 * j * LANES, 2 * LANES), 2 * LANES)]
+        columns = pl.ds(pl.multiple_of(j * LANES, LANES), LANES)
+        both = jnp.concatenate([gates[:, columns], ups[:, columns]], axis=1)
         both = jnp.dot(rows[...], both, preferred_element_type=F32)
         gate_out, up_out = both[:, :LANES], both[:, LANES:]
-        columns = pl.ds(pl.multiple_of(j * LANES, LANES), LANES)
         hidden[:, columns] = (gate_out * jax.nn.sigmoid(gate_out) * up_out).astype(BF16)
         return carry
 
-    lax.fori_loop(0, tiles, into, 0)
-    last.wait()
+    lax.fori_loop(0, gates.shape[1] // LANES, into, 0)
 
     def out_of(j, carry):
         columns = pl.ds(pl.multiple_of(2 * j * LANES, 2 * LANES), 2 * LANES)
-        result = jnp.dot(hidden[...], held[:, columns], preferred_element_type=F32).astype(BF16)
-        for k, out in enumerate(outs):
-            out[:, columns] = result[k * count : (k + 1) * count]
+        result = jnp.dot(hidden[...], downs[:, columns], preferred_element_type=F32).astype(BF16)
+        at = 0
+        for out in outs:
+            out[:, columns] = result[at : at + out.shape[0]]
+            at += out.shape[0]
         return carry
 
-    lax.fori_loop(0, down.shape[1] // (2 * LANES), out_of, 0)
+    lax.fori_loop(0, downs.shape[1] // (2 * LANES), out_of, 0)
 
 
 def all_rows(block, way):
-    from_left = moved(block, "x", 1)
-    from_right = moved(block, "x", -1)
-    far = moved(from_left if way > 0 else from_right, "x", way)
-    return block, from_left, from_right, far
+    if way:
+        from_left = moved(block, "x", 1)
+        from_right = moved(block, "x", -1)
+        far = moved(from_left if way > 0 else from_right, "x", way)
+        return (block, from_left, from_right), (far,)
+    half = block.shape[0] // 2
+    own_a, own_b = block[:half], block[half:]
+    left_a = moved(own_a, "x", 1)
+    right_b = moved(own_b, "x", -1)
+    left_b = moved(own_b, "x", 1)
+    right_a = moved(own_a, "x", -1)
+    far = moved(left_a, "x", 1), moved(right_b, "x", -1)
+    return (own_a, own_b, left_a, left_b, right_a, right_b), far
 
 
 def expert_parts(rows, weights):
-    count, wide = rows[0].shape
+    count, wide = sum(x.shape[0] for x in rows), rows[0].shape[1]
     part = weights[0].shape[1]
-    return call(
-        expert_body,
-        [shape((count, wide))] * 4,
-        [VMEM] * 4 + [pl.BlockSpec(memory_space=pltpu.HBM)] * 3,
-        scratch=[
-            pltpu.VMEM((4 * count, wide), BF16),
-            pltpu.VMEM((4 * count, part), BF16),
-            pltpu.VMEM((wide, 2 * part), BF16),
-            pltpu.VMEM((part, wide), BF16),
-            pltpu.SemaphoreType.DMA((2 * part // LANES + 1,)),
-        ],
-        flops=4 * count * 2 * wide * 3 * weights[0].shape[1],
+    run = call(
+        functools.partial(expert_body, len(rows)),
+        [shape(x.shape) for x in rows],
+        [VMEM] * (len(rows) + 3),
+        scratch=[pltpu.VMEM((count, wide), BF16), pltpu.VMEM((count, part), BF16)],
+        flops=count * 2 * wide * 3 * part,
         limit=EXPERT_LIMIT,
-    )(*rows, *weights)
+    )
+    return run(*rows, *weights)
 
 
 def added(*terms):
     return functools.reduce(jnp.add, [term.astype(F32) for term in terms]).astype(BF16)
 
 
-def summed(parts, way):
-    own, left, right, away = parts
-    relay = moved(away, "x", way)
-    low = moved(added(right, relay) if way > 0 else right, "x", 1)
-    high = moved(left if way > 0 else added(left, relay), "x", -1)
-    return added(own, low, high)
+def summed(near, away, way):
+    if way:
+        own, left, right = near
+        relay = moved(away[0], "x", way)
+        left, right = (left, added(right, relay)) if way > 0 else (added(left, relay), right)
+        low = moved(right, "x", 1)
+        high = moved(left, "x", -1)
+        return added(own, low, high)
+    own_a, own_b, left_a, left_b, right_a, right_b = near
+    low_b = moved(right_b, "x", 1)
+    high_a = moved(left_a, "x", -1)
+    relay_a = moved(away[0], "x", 1)
+    relay_b = moved(away[1], "x", -1)
+    low_a = moved(added(right_a, relay_a), "x", 1)
+    high_b = moved(added(left_b, relay_b), "x", -1)
+    return jnp.concatenate([added(own_a, low_a, high_a), added(own_b, low_b, high_b)])
 
 
 def exchanged(rows, devices):
@@ -378,9 +395,18 @@
     blocks = call(
         functools.partial(dispatch_body, experts, GROUPS),
         [shape((experts * (high - low), wide)) for low, high in GROUPS],
-        [VMEM] * 3,
+        [pl.BlockSpec(memory_space=pltpu.HBM)] * 2 + [VMEM],
+        scratch=[
+            pltpu.VMEM((n_tok, wide), BF16),
+            pltpu.VMEM((1, wide), F32),
+            pltpu.SemaphoreType.DMA((2,)),
+        ],
         flops=1 << 28,
-    )(tokens_into_experts, expert_norm_scale.reshape(1, -1), token_expert_index)
+    )(
+        pltpu.with_memory_space_constraint(tokens_into_experts, pltpu.HBM),
+        pltpu.with_memory_space_constraint(expert_norm_scale.reshape(1, -1), pltpu.HBM),
+        token_expert_index.T,
+    )
 
     def gathered(at, result, *total):
         low, high = GROUPS[at]
@@ -390,7 +416,7 @@
             shape((n_tok, wide), BF16 if last else F32),
             [VMEM] * (3 + len(total)),
             flops=1 << 28,
-        )(token_expert_index, chosen_expert_weight, result, *total)
+        )(token_expert_index.T, chosen_expert_weight.T, result, *total)
 
     packed, packed_wide = shape(PACKED), shape(PACKED, F32)
     first = exchanged(blocks[0], experts)
@@ -407,7 +433,7 @@
             functools.partial(double_body, ALL.index(axis), bit),
             [packed, packed_wide, packed_wide],
             [SMEM] + [VMEM] * (2 + len(before)),
-            flops=1 << 25,
+            flops=JOIN_FLOPS,
         )(where, got, whole, *before)
     axis, bit = bits[-1]
     got = flipped(sent, axis, bit)
@@ -426,15 +452,14 @@
         mine,
         arrived,
     )
-    second = exchanged(blocks[1], experts)
-    weights = [pltpu.with_memory_space_constraint(x, pltpu.HBM) for x in weights]
-    sums = []
-    for block, way in ((first, 1), (second, -1)):
-        parts = expert_parts(all_rows(block, way), weights)
-        sums.append(summed(parts, way))
-    first_back = exchanged(sums[0], experts)
-    second_back = exchanged(sums[1], experts)
-    expert_output = gathered(1, second_back, gathered(0, first_back))
+    total = ()
+    for at, way in enumerate(WAYS):
+        block = first if at == 0 else exchanged(blocks[at], experts)
+        near, far = all_rows(block, way)
+        near, far = expert_parts(near, weights), expert_parts(far, weights)
+        result = exchanged(summed(near, far, way), experts)
+        total = (gathered(at, result, *total),)
+    expert_output = total[0]
     return (mixed, expert_output)
 
 

time: 247 us -> 230 us (0.931)
  waiting for transfers between devices: 142 us -> 90.5 us
  starting transfers between devices: 55.2 us -> 69.5 us
  local copies, waits for them, and re-layouts: 8.39 us -> 21.9 us
  Pallas kernels: 34.6 us -> 40.2 us
    ppermute x12 -> x18, waiting for transfers between devices: 64.4 us -> 26.2 us  [moved(): return lax.ppermute(x, axis, [(k, (k + shift) % size) for k in range(size)])]
    all_to_all x4, waiting for transfers between devices: 43.5 us -> 26.8 us  [exchanged(): flat = lax.all_to_all(flat, YC, 0, 0, tiled=True)]
    ppermute x12 -> x18, starting transfers between devices: 15.7 us -> 28.4 us  [moved(): return lax.ppermute(x, axis, [(k, (k + shift) % size) for k in range(size)])]
    unnamed x24 -> x48, local copies, waits for them, and re-layouts: 2.68 us -> 12.2 us
    pallas_call x2 -> x4, Pallas kernels: 23.1 us -> 27.4 us  [expert_parts(): return run(*rows, *weights)]
    ppermute x7, waiting for transfers between devices: 33.7 us -> 37.5 us  [flipped(): lax.ppermute(x, axis, [(k, k ^ 1 << bit) for k in range(lax.axis_size(axi...]
    slice x0 -> x3, local copies, waits for them, and re-layouts: none -> 3.25 us  [all_rows(): own_a, own_b = (block[:half], block[half:])]
  transfers between devices with their start and end apart: 23 -> 29, of which waited for: 16 -> 13; matrix products, arithmetic and copies ran while one was open for 3% -> 5% of each run, Pallas kernels for 13% -> 16%
where the time goes in v1:
time: 230 us; the launch traced here: 228 us
  waiting for transfers between devices  90.5 us (39%)
  starting transfers between devices  69.5 us (30%)
  Pallas kernels  40.2 us (17%)
  local copies, waits for them, and re-layouts  21.9 us (10%)
  other arithmetic  4.63 us (2%)
    ppermute x7, waiting for transfers between devices, flipped(): lax.ppermute(x, axis, [(k, k ^ 1 << bit) for k in range(lax.axis_size(axi...  37.5 us
    all_to_all x4, starting transfers between devices, exchanged(): flat = lax.all_to_all(flat, YC, 0, 0, tiled=True)  31.2 us
    ppermute x18, starting transfers between devices, moved(): return lax.ppermute(x, axis, [(k, (k + shift) % size) for k in range(size)])  28.4 us
    pallas_call x4, Pallas kernels, expert_parts(): return run(*rows, *weights)  27.4 us
    all_to_all x4, waiting for transfers between devices, exchanged(): flat = lax.all_to_all(flat, YC, 0, 0, tiled=True)  26.8 us
    ppermute x18, waiting for transfers between devices, moved(): return lax.ppermute(x, axis, [(k, (k + shift) % size) for k in range(size)])  26.2 us
    unnamed x48, local copies, waits for them, and re-layouts  12.2 us
    ppermute x7, starting transfers between devices, flipped(): lax.ppermute(x, axis, [(k, k ^ 1 << bit) for k in range(lax.axis_size(axi...  9.95 us
  transfers between devices with their start and end apart: 29, of which 13 were waited for; matrix products, arithmetic and copies ran while one was open for 5% of the time, Pallas kernels for 16%

profile of v1, /device:TPU:8, one launch (start us, length us, event | category | flops | bytes accessed | tf_op | source)
XLA Modules:
  0.0 227.8 jit_solution(3213190900879080161)
XLA Ops:
  4.1 12.1 %all-to-all-start.2 = ((bf16[64,32,128]{2,1,0:T(8,128)(2,1)}), bf16[64,32,128]{2,1,0:T(8,128)(2,1)S(1)}, u32[]{:S(2)}, u32[]{:S(2)}) async-start(bf16[64,32,128]{2,1,0:T(8,128)(2,1)} %reshape.39), calls=%async_computation.2 | async-start | bytes 1048576 | tf_op jit(solution)/shard_map/all_to_all | solution.py:369
  25.4 8.4 %all-to-all-done.2 = bf16[64,32,128]{2,1,0:T(8,128)(2,1)S(1)} async-done(((bf16[64,32,128]{2,1,0:T(8,128)(2,1)}), bf16[64,32,128]{2,1,0:T(8,128)(2,1)S(1)}, u32[]{:S(2)}, u32[]{:S(2)}) %all-to-all-start.2) | async-done | bytes 524320 | tf_op jit(solution)/shard_map/all_to_all | solution.py:369
  33.7 6.0 %all-to-all-start = ((bf16[64,48,128]{2,1,0:T(8,128)(2,1)}), bf16[64,48,128]{2,1,0:T(8,128)(2,1)}, u32[]{:S(2)}, u32[]{:S(2)}) async-start(bf16[64,48,128]{2,1,0:T(8,128)(2,1)} %reshape.36), calls=%async_computation | async-start | bytes 1572864 | tf_op jit(solution)/shard_map/all_to_all | solution.py:369
  46.1 4.0 %collective-permute-done.2.got_ref = bf16[272,256]{1,0:T(8,128)(2,1)S(1)} collective-permute-done((bf16[272,256]{1,0:T(8,128)(2,1)S(1)}, bf16[272,256]{1,0:T(8,128)(2,1)S(1)}, u32[]{:S(2)}, u32[]{:S(2)}) %collective-permute-start.2) | collective-permute-done | bytes 139296 | tf_op jit(solution)/shard_map/ppermute | solution.py:216
  52.8 4.9 %collective-permute-done.19.refs_1_ = bf16[128,2048]{1,0:T(8,128)(2,1)S(1)} collective-permute-done((bf16[128,2048]{1,0:T(8,128)(2,1)S(1)}, bf16[128,2048]{1,0:T(8,128)(2,1)S(1)}, u32[]{:S(2)}, u32[]{:S(2)}) %collective-permute-start.19) | collective-permute-done | bytes 524320 | tf_op jit(solution)/shard_map/ppermute | solution.py:212
  58.1 4.8 %all-to-all-done = bf16[64,48,128]{2,1,0:T(8,128)(2,1)} async-done(((bf16[64,48,128]{2,1,0:T(8,128)(2,1)}), bf16[64,48,128]{2,1,0:T(8,128)(2,1)}, u32[]{:S(2)}, u32[]{:S(2)}) %all-to-all-start) | async-done | bytes 786464 | tf_op jit(solution)/shard_map/all_to_all | solution.py:369
  64.9 2.8 %collective-permute-start.10 = (bf16[96,2048]{1,0:T(8,128)(2,1)S(1)}, bf16[96,2048]{1,0:T(8,128)(2,1)}, u32[]{:S(2)}, u32[]{:S(2)}) collective-permute-start(bf16[96,2048]{1,0:T(8,128)(2,1)S(1)} %slice.15.refs_1_), channel_id=1, source_target_pairs={{0,3},{1,0},{2,1},{3,2},{4,7},{5,4},{6,5},{7,6},{8,11},{9,8},{10,9... | collective-permute-start | bytes 1179656 | tf_op jit(solution)/shard_map/ppermute | solution.py:212
  69.8 2.8 %collective-permute-start.9 = (bf16[96,2048]{1,0:T(8,128)(2,1)S(1)}, bf16[96,2048]{1,0:T(8,128)(2,1)S(1)}, u32[]{:S(2)}, u32[]{:S(2)}) collective-permute-start(bf16[96,2048]{1,0:T(8,128)(2,1)S(1)} %slice.13.refs_0_), channel_id=1, source_target_pairs={{0,3},{1,0},{2,1},{3,2},{4,7},{5,4},{6,5},{7,6},{8,11},{9,8},{10,9... | collective-permute-start | bytes 1179656 | tf_op jit(solution)/shard_map/ppermute | solution.py:212
  78.7 7.3 %shard_map.169 = (bf16[128,2048]{1,0:T(8,128)(2,1)S(1)}, bf16[128,2048]{1,0:T(8,128)(2,1)S(1)}, bf16[128,2048]{1,0:T(8,128)(2,1)S(1)}) custom-call(bf16[128,2048]{1,0:T(8,128)(2,1)S(1)} %reshape.40.refs_0_, bf16[128,2048]{1,0:T(8,128)(2,1)S(1)} %collective-permute-done.19.refs_1_, bf16[128,2048]{1,0:T(8,128)(2,1)S(1)} %collective-permute-done.20.refs_2_, ...), custom_call_target="tpu_custom_call" | custom-call | flops 4227858432 | bytes 16515072 | tf_op jit(solution)/shard_map/pallas_call | solution.py:341
  86.7 4.3 %shard_map.170 = bf16[128,2048]{1,0:T(8,128)(2,1)S(1)} custom-call(bf16[128,2048]{1,0:T(8,128)(2,1)S(1)} %collective-permute-done.21.refs_0_, bf16[2048,896]{1,0:T(8,128)(2,1)S(1)} %bitcast.12, bf16[2048,896]{1,0:T(8,128)(2,1)S(1)} %bitcast.16, bf16[896,2048]{1,0:T(8,128)(2,1)S(1)} %bitcast.20), custom_call_target="tpu_custom_call" | custom-call | flops 1409286144 | bytes 5505024 | tf_op jit(solution)/shard_map/pallas_call | solution.py:341
  93.1 3.0 %collective-permute-start.12 = (bf16[96,2048]{1,0:T(8,128)(2,1)}, bf16[96,2048]{1,0:T(8,128)(2,1)S(1)}, u32[]{:S(2)}, u32[]{:S(2)}) collective-permute-start(bf16[96,2048]{1,0:T(8,128)(2,1)} %collective-permute-done.10.refs_5_), channel_id=1, source_target_pairs={{0,3},{1,0},{2,1},{3,2},{4,7},{5,4},{6,5},{7,6},{8,11},{9,8},{10,9... | collective-permute-start | bytes 1179656 | tf_op jit(solution)/shard_map/ppermute | solution.py:212
  96.1 10.7 %shard_map.167 = (bf16[96,2048]{1,0:T(8,128)(2,1)S(1)}, bf16[96,2048]{1,0:T(8,128)(2,1)S(1)}, bf16[96,2048]{1,0:T(8,128)(2,1)S(1)}, bf16[96,2048]{1,0:T(8,128)(2...) custom-call(bf16[96,2048]{1,0:T(8,128)(2,1)S(1)} %slice.13.refs_0_, ...), custom_call_target="tpu_custom_call" | custom-call | flops 6341787648 | bytes 24772608 | tf_op jit(solution)/shard_map/pallas_call | solution.py:341
  106.8 3.3 %collective-permute-start.15 = (bf16[96,2048]{1,0:T(8,128)(2,1)S(1)}, bf16[96,2048]{1,0:T(8,128)(2,1)S(1)}, u32[]{:S(2)}, u32[]{:S(2)}) collective-permute-start(bf16[96,2048]{1,0:T(8,128)(2,1)S(1)} %get-tuple-element.53), channel_id=1, source_target_pairs={{0,3},{1,0},{2,1},{3,2},{4,7},{5,4},{6,5},{7,6},{8,11},{9,8},{10,9... | collective-permute-start | bytes 1179656 | tf_op jit(solution)/shard_map/ppermute | solution.py:212
  110.1 4.2 %collective-permute-done.12.refs_1_ = bf16[96,2048]{1,0:T(8,128)(2,1)S(1)} collective-permute-done((bf16[96,2048]{1,0:T(8,128)(2,1)}, bf16[96,2048]{1,0:T(8,128)(2,1)S(1)}, u32[]{:S(2)}, u32[]{:S(2)}) %collective-permute-start.12) | collective-permute-done | bytes 393248 | tf_op jit(solution)/shard_map/ppermute | solution.py:212
  114.3 5.1 %shard_map.168 = (bf16[96,2048]{1,0:T(8,128)(2,1)S(1)}, bf16[96,2048]{1,0:T(8,128)(2,1)S(1)}) custom-call(bf16[96,2048]{1,0:T(8,128)(2,1)S(1)} %collective-permute-done.11.refs_0_, bf16[96,2048]{1,0:T(8,128)(2,1)S(1)} %collective-permute-done.12.refs_1_, bf16[2048,896]{1,0:T(8,128)(2,1)S(1)} %bitcast.14, bf16[2048,896]{1,0:T(8,128)(2,1)S(1)} %bitcast.18, ...), custom_call_target="tpu_custom_call" | custom-call | flops 2113929216 | bytes 8257536 | tf_op jit(solution)/shard_map/pallas_call | solution.py:341
  119.5 3.2 %collective-permute-start.17 = (bf16[96,2048]{1,0:T(8,128)(2,1)S(1)}, bf16[96,2048]{1,0:T(8,128)(2,1)S(1)}, u32[]{:S(2)}, u32[]{:S(2)}) collective-permute-start(bf16[96,2048]{1,0:T(8,128)(2,1)S(1)} %get-tuple-element.57), channel_id=1, source_target_pairs={{0,3},{1,0},{2,1},{3,2},{4,7},{5,4},{6,5},{7,6},{8,11},{9,8},{10,9... | collective-permute-start | bytes 1179656 | tf_op jit(solution)/shard_map/ppermute | solution.py:212
  122.8 7.2 %collective-permute-done.13 = bf16[96,2048]{1,0:T(8,128)(2,1)S(1)} collective-permute-done((bf16[96,2048]{1,0:T(8,128)(2,1)S(1)}, bf16[96,2048]{1,0:T(8,128)(2,1)S(1)}, u32[]{:S(2)}, u32[]{:S(2)}) %collective-permute-start.13) | collective-permute-done | bytes 393248 | tf_op jit(solution)/shard_map/ppermute | solution.py:212
  136.4 9.7 %collective-permute-done.23 = bf16[128,2048]{1,0:T(8,128)(2,1)S(1)} collective-permute-done((bf16[128,2048]{1,0:T(8,128)(2,1)S(1)}, bf16[128,2048]{1,0:T(8,128)(2,1)S(1)}, u32[]{:S(2)}, u32[]{:S(2)}) %collective-permute-start.23) | collective-permute-done | bytes 524320 | tf_op jit(solution)/shard_map/ppermute | solution.py:212
  149.4 7.1 %all-to-all-start.3 = ((bf16[64,32,128]{2,1,0:T(8,128)(2,1)}), bf16[64,32,128]{2,1,0:T(8,128)(2,1)S(1)}, u32[]{:S(2)}, u32[]{:S(2)}) async-start(bf16[64,32,128]{2,1,0:T(8,128)(2,1)} %reshape.41), calls=%async_computation.3 | async-start | bytes 1048576 | tf_op jit(solution)/shard_map/all_to_all | solution.py:369
  160.4 13.6 %all-to-all-done.3 = bf16[64,32,128]{2,1,0:T(8,128)(2,1)S(1)} async-done(((bf16[64,32,128]{2,1,0:T(8,128)(2,1)}), bf16[64,32,128]{2,1,0:T(8,128)(2,1)S(1)}, u32[]{:S(2)}, u32[]{:S(2)}) %all-to-all-start.3) | async-done | bytes 524320 | tf_op jit(solution)/shard_map/all_to_all | solution.py:369
  174.0 6.0 %all-to-all-start.1 = ((bf16[64,48,128]{2,1,0:T(8,128)(2,1)}), bf16[64,48,128]{2,1,0:T(8,128)(2,1)}, u32[]{:S(2)}, u32[]{:S(2)}) async-start(bf16[64,48,128]{2,1,0:T(8,128)(2,1)} %reshape.37), calls=%async_computation.1 | async-start | bytes 1572864 | tf_op jit(solution)/shard_map/all_to_all | solution.py:369
  183.2 22.7 %collective-permute-done.4.got_ref = bf16[272,256]{1,0:T(8,128)(2,1)S(1)} collective-permute-done((bf16[272,256]{1,0:T(8,128)(2,1)S(1)}, bf16[272,256]{1,0:T(8,128)(2,1)S(1)}, u32[]{:S(2)}, u32[]{:S(2)}) %collective-permute-start.4) | collective-permute-done | bytes 139296 | tf_op jit(solution)/shard_map/ppermute | solution.py:216
  207.3 3.8 %collective-permute-start.5 = (bf16[272,256]{1,0:T(8,128)(2,1)S(1)}, bf16[272,256]{1,0:T(8,128)(2,1)S(1)}, u32[]{:S(2)}, u32[]{:S(2)}) collective-permute-start(bf16[272,256]{1,0:T(8,128)(2,1)S(1)} %get-tuple-element.45), channel_id=1, source_target_pairs={{0,128},{32,160},{64,192},{96,224},{128,0},{160,32},{192,64},{224,... | collective-permute-start | bytes 417800 | tf_op jit(solution)/shard_map/ppermute | solution.py:216
  211.1 8.2 %collective-permute-done.5.got_ref = bf16[272,256]{1,0:T(8,128)(2,1)S(1)} collective-permute-done((bf16[272,256]{1,0:T(8,128)(2,1)S(1)}, bf16[272,256]{1,0:T(8,128)(2,1)S(1)}, u32[]{:S(2)}, u32[]{:S(2)}) %collective-permute-start.5) | collective-permute-done | bytes 139296 | tf_op jit(solution)/shard_map/ppermute | solution.py:216
  (115 shorter events, 61.6 us)
Async XLA Ops:
  4.1 29.6 %all-to-all-start.2 = ((bf16[64,32,128]{2,1,0:T(8,128)(2,1)}), bf16[64,32,128]{2,1,0:T(8,128)(2,1)S(1)}, u32[]{:S(2)}, u32[]{:S(2)}) async-start(bf16[64,32,128]{2,1,0:T(8,128)(2,1)} %reshape.39), calls=%async_computation.2 | async-start | bytes 1048576 | tf_op jit(solution)/shard_map/all_to_all | solution.py:369
  23.6 16.2 %collective-permute-start.1 = (bf16[272,256]{1,0:T(8,128)(2,1)S(1)}, bf16[272,256]{1,0:T(8,128)(2,1)S(1)}, u32[]{:S(2)}, u32[]{:S(2)}) collective-permute-start(bf16[272,256]{1,0:T(8,128)(2,1)S(1)} %get-tuple-element.34), channel_id=1, source_target_pairs={{0,8},{8,0},{16,24},{24,16},{1,9},{9,1},{17,25},{25,17},{2,10},{10... | collective-permute-start | bytes 417800 | tf_op jit(solution)/shard_map/ppermute | solution.py:216
  33.7 29.1 %all-to-all-start = ((bf16[64,48,128]{2,1,0:T(8,128)(2,1)}), bf16[64,48,128]{2,1,0:T(8,128)(2,1)}, u32[]{:S(2)}, u32[]{:S(2)}) async-start(bf16[64,48,128]{2,1,0:T(8,128)(2,1)} %reshape.36), calls=%async_computation | async-start | bytes 1572864 | tf_op jit(solution)/shard_map/all_to_all | solution.py:369
  42.8 15.0 %collective-permute-start.19 = (bf16[128,2048]{1,0:T(8,128)(2,1)S(1)}, bf16[128,2048]{1,0:T(8,128)(2,1)S(1)}, u32[]{:S(2)}, u32[]{:S(2)}) collective-permute-start(bf16[128,2048]{1,0:T(8,128)(2,1)S(1)} %reshape.40.refs_0_), channel_id=1, source_target_pairs={{0,1},{1,2},{2,3},{3,0},{4,5},{5,6},{6,7},{7,4},{8,9},{9,10},{10,1... | collective-permute-start | bytes 1572872 | tf_op jit(solution)/shard_map/ppermute | solution.py:212
  44.4 25.4 %collective-permute-start.20 = (bf16[128,2048]{1,0:T(8,128)(2,1)S(1)}, bf16[128,2048]{1,0:T(8,128)(2,1)S(1)}, u32[]{:S(2)}, u32[]{:S(2)}) collective-permute-start(bf16[128,2048]{1,0:T(8,128)(2,1)S(1)} %reshape.40.refs_0_), channel_id=1, source_target_pairs={{0,3},{1,0},{2,1},{3,2},{4,7},{5,4},{6,5},{7,6},{8,11},{9,8},{10,9... | collective-permute-start | bytes 1572872 | tf_op jit(solution)/shard_map/ppermute | solution.py:212
  57.8 28.2 %collective-permute-start.21 = (bf16[128,2048]{1,0:T(8,128)(2,1)S(1)}, bf16[128,2048]{1,0:T(8,128)(2,1)S(1)}, u32[]{:S(2)}, u32[]{:S(2)}) collective-permute-start(bf16[128,2048]{1,0:T(8,128)(2,1)S(1)} %collective-permute-done.19.refs_1_), channel_id=1, source_target_pairs={{0,1},{1,2},{2,3},{3,0},{4,5},{5,6},{6,7},{7,4},{8,9},{9,10},{10,1... | collective-permute-start | bytes 1572872 | tf_op jit(solution)/shard_map/ppermute | solution.py:212
  64.9 26.0 %collective-permute-start.10 = (bf16[96,2048]{1,0:T(8,128)(2,1)S(1)}, bf16[96,2048]{1,0:T(8,128)(2,1)}, u32[]{:S(2)}, u32[]{:S(2)}) collective-permute-start(bf16[96,2048]{1,0:T(8,128)(2,1)S(1)} %slice.15.refs_1_), channel_id=1, source_target_pairs={{0,3},{1,0},{2,1},{3,2},{4,7},{5,4},{6,5},{7,6},{8,11},{9,8},{10,9... | collective-permute-start | bytes 1179656 | tf_op jit(solution)/shard_map/ppermute | solution.py:212
  67.8 25.3 %collective-permute-start.8 = (bf16[96,2048]{1,0:T(8,128)(2,1)S(1)}, bf16[96,2048]{1,0:T(8,128)(2,1)}, u32[]{:S(2)}, u32[]{:S(2)}) collective-permute-start(bf16[96,2048]{1,0:T(8,128)(2,1)S(1)} %slice.15.refs_1_), channel_id=1, source_target_pairs={{0,1},{1,2},{2,3},{3,0},{4,5},{5,6},{6,7},{7,4},{8,9},{9,10},{10,1... | collective-permute-start | bytes 1179656 | tf_op jit(solution)/shard_map/ppermute | solution.py:212
  68.9 23.9 %collective-permute-start.7 = (bf16[96,2048]{1,0:T(8,128)(2,1)S(1)}, bf16[96,2048]{1,0:T(8,128)(2,1)S(1)}, u32[]{:S(2)}, u32[]{:S(2)}) collective-permute-start(bf16[96,2048]{1,0:T(8,128)(2,1)S(1)} %slice.13.refs_0_), channel_id=1, source_target_pairs={{0,1},{1,2},{2,3},{3,0},{4,5},{5,6},{6,7},{7,4},{8,9},{9,10},{10,1... | collective-permute-start | bytes 1179656 | tf_op jit(solution)/shard_map/ppermute | solution.py:212
  69.8 26.3 %collective-permute-start.9 = (bf16[96,2048]{1,0:T(8,128)(2,1)S(1)}, bf16[96,2048]{1,0:T(8,128)(2,1)S(1)}, u32[]{:S(2)}, u32[]{:S(2)}) collective-permute-start(bf16[96,2048]{1,0:T(8,128)(2,1)S(1)} %slice.13.refs_0_), channel_id=1, source_target_pairs={{0,3},{1,0},{2,1},{3,2},{4,7},{5,4},{6,5},{7,6},{8,11},{9,8},{10,9... | collective-permute-start | bytes 1179656 | tf_op jit(solution)/shard_map/ppermute | solution.py:212
  86.0 94.1 %collective-permute-start.3 = (bf16[272,256]{1,0:T(8,128)(2,1)}, bf16[272,256]{1,0:T(8,128)(2,1)S(1)}, u32[]{:S(2)}, u32[]{:S(2)}) collective-permute-start(bf16[272,256]{1,0:T(8,128)(2,1)} %get-tuple-element.39), channel_id=1, source_target_pairs={{0,32},{32,0},{64,96},{96,64},{128,160},{160,128},{192,224},{224,1... | collective-permute-start | bytes 417800 | tf_op jit(solution)/shard_map/ppermute | solution.py:216
  91.0 43.0 %collective-permute-start.24 = (bf16[128,2048]{1,0:T(8,128)(2,1)S(1)}, bf16[128,2048]{1,0:T(8,128)(2,1)S(1)}, u32[]{:S(2)}, u32[]{:S(2)}) collective-permute-start(bf16[128,2048]{1,0:T(8,128)(2,1)S(1)} %get-tuple-element.61), channel_id=1, source_target_pairs={{0,3},{1,0},{2,1},{3,2},{4,7},{5,4},{6,5},{7,6},{8,11},{9,8},{10,9... | collective-permute-start | bytes 1572872 | tf_op jit(solution)/shard_map/ppermute | solution.py:212
  92.8 14.0 %collective-permute-start.11 = (bf16[96,2048]{1,0:T(8,128)(2,1)S(1)}, bf16[96,2048]{1,0:T(8,128)(2,1)S(1)}, u32[]{:S(2)}, u32[]{:S(2)}) collective-permute-start(bf16[96,2048]{1,0:T(8,128)(2,1)S(1)} %collective-permute-done.7.refs_2_), channel_id=1, source_target_pairs={{0,1},{1,2},{2,3},{3,0},{4,5},{5,6},{6,7},{7,4},{8,9},{9,10},{10,1... | collective-permute-start | bytes 1179656 | tf_op jit(solution)/shard_map/ppermute | solution.py:212
  93.1 21.2 %collective-permute-start.12 = (bf16[96,2048]{1,0:T(8,128)(2,1)}, bf16[96,2048]{1,0:T(8,128)(2,1)S(1)}, u32[]{:S(2)}, u32[]{:S(2)}) collective-permute-start(bf16[96,2048]{1,0:T(8,128)(2,1)} %collective-permute-done.10.refs_5_), channel_id=1, source_target_pairs={{0,3},{1,0},{2,1},{3,2},{4,7},{5,4},{6,5},{7,6},{8,11},{9,8},{10,9... | collective-permute-start | bytes 1179656 | tf_op jit(solution)/shard_map/ppermute | solution.py:212
  96.1 23.4 %collective-permute-start.22 = (bf16[128,2048]{1,0:T(8,128)(2,1)S(1)}, bf16[128,2048]{1,0:T(8,128)(2,1)S(1)}, u32[]{:S(2)}, u32[]{:S(2)}) collective-permute-start(bf16[128,2048]{1,0:T(8,128)(2,1)S(1)} %shard_map.170), channel_id=1, source_target_pairs={{0,1},{1,2},{2,3},{3,0},{4,5},{5,6},{6,7},{7,4},{8,9},{9,10},{10,1... | collective-permute-start | bytes 1572872 | tf_op jit(solution)/shard_map/ppermute | solution.py:212
  106.8 49.7 %collective-permute-start.15 = (bf16[96,2048]{1,0:T(8,128)(2,1)S(1)}, bf16[96,2048]{1,0:T(8,128)(2,1)S(1)}, u32[]{:S(2)}, u32[]{:S(2)}) collective-permute-start(bf16[96,2048]{1,0:T(8,128)(2,1)S(1)} %get-tuple-element.53), channel_id=1, source_target_pairs={{0,3},{1,0},{2,1},{3,2},{4,7},{5,4},{6,5},{7,6},{8,11},{9,8},{10,9... | collective-permute-start | bytes 1179656 | tf_op jit(solution)/shard_map/ppermute | solution.py:212
  130.1 16.0 %collective-permute-start.23 = (bf16[128,2048]{1,0:T(8,128)(2,1)S(1)}, bf16[128,2048]{1,0:T(8,128)(2,1)S(1)}, u32[]{:S(2)}, u32[]{:S(2)}) collective-permute-start(bf16[128,2048]{1,0:T(8,128)(2,1)S(1)} %add_convert_fusion.1), channel_id=1, source_target_pairs={{0,1},{1,2},{2,3},{3,0},{4,5},{5,6},{6,7},{7,4},{8,9},{9,10},{10,1... | collective-permute-start | bytes 1572872 | tf_op jit(solution)/shard_map/ppermute | solution.py:212
  130.9 26.9 %collective-permute-start.16 = (bf16[96,2048]{1,0:T(8,128)(2,1)S(1)}, bf16[96,2048]{1,0:T(8,128)(2,1)}, u32[]{:S(2)}, u32[]{:S(2)}) collective-permute-start(bf16[96,2048]{1,0:T(8,128)(2,1)S(1)} %get-tuple-element.55), channel_id=1, source_target_pairs={{0,1},{1,2},{2,3},{3,0},{4,5},{5,6},{6,7},{7,4},{8,9},{9,10},{10,1... | collective-permute-start | bytes 1179656 | tf_op jit(solution)/shard_map/ppermute | solution.py:212
  134.0 22.7 %collective-permute-start.14 = (bf16[96,2048]{1,0:T(8,128)(2,1)}, bf16[96,2048]{1,0:T(8,128)(2,1)}, u32[]{:S(2)}, u32[]{:S(2)}) collective-permute-start(bf16[96,2048]{1,0:T(8,128)(2,1)} %add_convert_fusion.5), channel_id=1, source_target_pairs={{0,1},{1,2},{2,3},{3,0},{4,5},{5,6},{6,7},{7,4},{8,9},{9,10},{10,1... | collective-permute-start | bytes 1179656 | tf_op jit(solution)/shard_map/ppermute | solution.py:212
  146.1 11.8 %collective-permute-start.18 = (bf16[96,2048]{1,0:T(8,128)(2,1)}, bf16[96,2048]{1,0:T(8,128)(2,1)}, u32[]{:S(2)}, u32[]{:S(2)}) collective-permute-start(bf16[96,2048]{1,0:T(8,128)(2,1)} %add_convert_fusion.3), channel_id=1, source_target_pairs={{0,3},{1,0},{2,1},{3,2},{4,7},{5,4},{6,5},{7,6},{8,11},{9,8},{10,9... | collective-permute-start | bytes 1179656 | tf_op jit(solution)/shard_map/ppermute | solution.py:212
  149.4 24.6 %all-to-all-start.3 = ((bf16[64,32,128]{2,1,0:T(8,128)(2,1)}), bf16[64,32,128]{2,1,0:T(8,128)(2,1)S(1)}, u32[]{:S(2)}, u32[]{:S(2)}) async-start(bf16[64,32,128]{2,1,0:T(8,128)(2,1)} %reshape.41), calls=%async_computation.3 | async-start | bytes 1048576 | tf_op jit(solution)/shard_map/all_to_all | solution.py:369
  174.0 50.7 %all-to-all-start.1 = ((bf16[64,48,128]{2,1,0:T(8,128)(2,1)}), bf16[64,48,128]{2,1,0:T(8,128)(2,1)}, u32[]{:S(2)}, u32[]{:S(2)}) async-start(bf16[64,48,128]{2,1,0:T(8,128)(2,1)} %reshape.37), calls=%async_computation.1 | async-start | bytes 1572864 | tf_op jit(solution)/shard_map/all_to_all | solution.py:369
  180.8 25.1 %collective-permute-start.4 = (bf16[272,256]{1,0:T(8,128)(2,1)S(1)}, bf16[272,256]{1,0:T(8,128)(2,1)S(1)}, u32[]{:S(2)}, u32[]{:S(2)}) collective-permute-start(bf16[272,256]{1,0:T(8,128)(2,1)S(1)} %get-tuple-element.42), channel_id=1, source_target_pairs={{0,64},{32,96},{64,0},{96,32},{128,192},{160,224},{192,128},{224,1... | collective-permute-start | bytes 417800 | tf_op jit(solution)/shard_map/ppermute | solution.py:216
  207.3 12.0 %collective-permute-start.5 = (bf16[272,256]{1,0:T(8,128)(2,1)S(1)}, bf16[272,256]{1,0:T(8,128)(2,1)S(1)}, u32[]{:S(2)}, u32[]{:S(2)}) collective-permute-start(bf16[272,256]{1,0:T(8,128)(2,1)S(1)} %get-tuple-element.45), channel_id=1, source_target_pairs={{0,128},{32,160},{64,192},{96,224},{128,0},{160,32},{192,64},{224,... | collective-permute-start | bytes 417800 | tf_op jit(solution)/shard_map/ppermute | solution.py:216
  (29 other events, 278.4 us)
